TPU v7x, 32 devices: a whole 2x2x4 slice. The times are simulated.
32 devices in a mesh: ep: 8 (over z, y), tp: 4 (over x, core).
Axes of the slice: x: 2, y: 2, z: 4, core: 2. Of those that a mesh axis runs over, the one named last changes fastest.
Arguments:
- mixer_input: bfloat16 [4096, 2048], P('ep'), may hold values from -6 to 6
- mixer_gain: bfloat16 [2048], replicated, may hold values from 0.099609375 to 1.8984375
- pool_in: bfloat16 [2048, 1024], P(None, 'tp'), may hold values from -0.125 to 0.125
- pool_map: bfloat16 [4, 256, 256], P('tp'), may hold values from -0.375 to 0.375
- pool_scale: bfloat16 [1024], P('tp'), may hold values from 0.099609375 to 1.8984375
- pool_out: bfloat16 [1024, 2048], P('tp'), may hold values from -0.1875 to 0.1875
- expert_input: bfloat16 [3072, 2048], P('ep'), may hold values from -6 to 6
- expert_gain: bfloat16 [2048], replicated, may hold values from 0.099609375 to 1.8984375
- group_router: bfloat16 [2048, 4], replicated, may hold values from -0.125 to 0.125
- expert_router: bfloat16 [2048, 8], replicated, may hold values from -0.125 to 0.125
- routes: int32 [3072, 2], P('ep'), may hold values from 0 to 7, all different within a row; in each aligned block of 96 rows (0 to 95, 96 to 191, ...) at most 48 rows name the same one
- gate_weight: bfloat16 [8, 2048, 1024], P('ep', None, 'tp'), may hold values from -0.125 to 0.125
- up_weight: bfloat16 [8, 2048, 1024], P('ep', None, 'tp'), may hold values from -0.125 to 0.125
- down_weight: bfloat16 [8, 1024, 2048], P('ep', 'tp'), may hold values from -0.1875 to 0.1875
Outputs:
- mixer_output: bfloat16 [4096, 2048], P(('ep', 'tp'))
- expert_output: bfloat16 [3072, 2048], P(('ep', 'tp'))
Inputs may be any that keep to these rules, and one draw needn't show every extreme that they name: `routes`: each row names two different experts. In each aligned block of 96 rows no expert is named more than 48 times, a bound that some block reaches.
All inputs are finite; a program needn't handle non-finite values.
Results may differ from a plain program's by a relative error of at most 0.01.
Values may be sent and summed in bfloat16 or wider, within the bound.
A program may use at most 64 MiB of HBM per device.

v0:
```python
import jax
import jax.numpy as jnp
from jax import lax
from jax.sharding import PartitionSpec as P

RIM = 15
EPS = 1e-06


def passed_along(value, axis, steps):
    count = lax.axis_size(axis)
    leading, last = (max(0, -steps), min(count, count - steps))
    return lax.ppermute(value, axis, [(source, source + steps) for source in range(leading, last)])


def norm_rows(values, gain):
    floats = values.astype(jnp.float32)
    scale = lax.rsqrt(jnp.mean(floats * floats, axis=-1, keepdims=True) + EPS)
    return (floats * scale * gain.astype(jnp.float32)).astype(jnp.bfloat16)


def route_weights(rows, group_router, expert_router, route_rows):
    group_logits = jnp.dot(rows, group_router, preferred_element_type=jnp.float32)
    expert_logits = jnp.dot(rows, expert_router, preferred_element_type=jnp.float32)
    groups = group_logits.shape[1]
    experts = expert_logits.shape[1]
    member = (
        jnp.arange(experts, dtype=jnp.int32)[:, None] // (experts // groups)
        == jnp.arange(groups, dtype=jnp.int32)[None, :]
    ).astype(jnp.float32)
    group_exp = jnp.exp(group_logits)
    group_prob = group_exp / jnp.sum(group_exp, axis=1, keepdims=True)
    expert_exp = jnp.exp(expert_logits)
    within = jnp.dot(expert_exp, member, precision=lax.Precision.HIGHEST)
    prob = expert_exp * jnp.dot(group_prob / within, member.T, precision=lax.Precision.HIGHEST)
    chosen = (route_rows[:, :, None] == jnp.arange(experts, dtype=jnp.int32)[None, None, :]).astype(
        jnp.float32
    )
    picked = jnp.sum(chosen * prob[:, None, :], axis=2)
    return picked / jnp.sum(picked, axis=1, keepdims=True)


def mixer_half(mixer_input, mixer_gain, pool_in, pool_map, pool_scale, pool_out):
    normed = norm_rows(mixer_input, mixer_gain)
    pooled_in = jnp.dot(normed, pool_in, preferred_element_type=jnp.float32).astype(jnp.bfloat16)
    local_rows = pooled_in.shape[0]
    groups_here = pool_map.shape[0]
    channels = pool_map.shape[1]
    border = passed_along(pooled_in[local_rows - RIM :], "ep", 1)
    padded = jnp.concatenate([border, pooled_in], axis=0).astype(jnp.float32)
    padded = padded.reshape(local_rows + RIM, groups_here, channels)
    leading = lax.axis_index("tp") * groups_here
    windows = jnp.left_shift(jnp.int32(2), leading + jnp.arange(groups_here, dtype=jnp.int32))
    window_sum = jnp.zeros((local_rows, groups_here, channels), jnp.float32)
    for offset in range(RIM + 1):
        active = (offset < windows).astype(jnp.float32)
        window_sum = (
            window_sum + padded[RIM - offset : RIM - offset + local_rows] * active[None, :, None]
        )
    position = lax.axis_index("ep") * local_rows + jnp.arange(local_rows, dtype=jnp.int32)
    counts_here = jnp.minimum(position[:, None] + 1, windows[None, :]).astype(jnp.float32)
    pooled = (window_sum / counts_here[:, :, None] - padded[RIM:]).astype(jnp.bfloat16)
    mapped = jnp.einsum("tgc,gce->tge", pooled, pool_map, preferred_element_type=jnp.float32)
    mixed_rows = (
        mapped.reshape(local_rows, groups_here * channels) * pool_scale.astype(jnp.float32)
    ).astype(jnp.bfloat16)
    return lax.psum_scatter(
        jnp.dot(mixed_rows, pool_out, preferred_element_type=jnp.float32).astype(jnp.bfloat16),
        "tp",
        scatter_dimension=0,
        tiled=True,
    )


def slot_positions(route_rows, blocks, experts):
    flat = route_rows.reshape(blocks, -1)
    onehot = (flat[:, :, None] == jnp.arange(experts, dtype=jnp.int32)[None, None, :]).astype(
        jnp.int32
    )
    before = jnp.cumsum(onehot, axis=1) - onehot
    return (jnp.sum(before * onehot, axis=2), flat)


def dispatch_rows(normed, route_rows, blocks, slots_each, experts):
    block_len = normed.shape[0] // blocks
    positions, flat = slot_positions(route_rows, blocks, experts)
    block_index = jnp.arange(blocks, dtype=jnp.int32)[:, None]
    slot_index = block_index * slots_each + positions
    token_index = block_index * block_len + jnp.arange(2 * block_len, dtype=jnp.int32)[None, :] // 2
    table = jnp.full((blocks * slots_each, experts), -1, jnp.int32)
    table = table.at[slot_index.reshape(-1), flat.reshape(-1)].set(token_index.reshape(-1))
    fetched = normed[jnp.maximum(table, 0)]
    return jnp.where((table >= 0)[:, :, None], fetched, jnp.zeros_like(fetched))


def expert_half(
    expert_input,
    expert_gain,
    group_router,
    expert_router,
    routes,
    gate_weight,
    up_weight,
    down_weight,
):
    normed = norm_rows(expert_input, expert_gain)
    tp_count = lax.axis_size("tp")
    tp_place = lax.axis_index("tp")
    experts = expert_router.shape[1]
    block_len = normed.shape[0] // tp_count
    slots_each = 4 * block_len // experts
    own_rows = lax.dynamic_slice_in_dim(normed, tp_place * block_len, block_len, 0)
    own_routes = lax.dynamic_slice_in_dim(routes, tp_place * block_len, block_len, 0)
    sending = dispatch_rows(own_rows, own_routes, 1, slots_each, experts)
    arrived = lax.all_to_all(sending, "ep", split_axis=1, concat_axis=1, tiled=True)
    received = lax.all_gather(arrived, "tp", axis=0, tiled=True)
    held = gate_weight.shape[0]
    model = received.shape[2]
    portion = received
    portion = portion.reshape(lax.axis_size("tp") * slots_each, -1, held, model)
    gate = jnp.einsum("csed,edh->cseh", portion, gate_weight, preferred_element_type=jnp.float32)
    upward = jnp.einsum("csed,edh->cseh", portion, up_weight, preferred_element_type=jnp.float32)
    hidden = (jax.nn.silu(gate) * upward).astype(jnp.bfloat16)
    result = jnp.einsum("cseh,ehd->csed", hidden, down_weight, preferred_element_type=jnp.float32)
    summed = lax.psum_scatter(
        result.reshape(lax.axis_size("tp") * slots_each, -1, model).astype(jnp.bfloat16),
        "tp",
        scatter_dimension=0,
        tiled=True,
    )
    returned = lax.all_to_all(summed, "ep", split_axis=1, concat_axis=1, tiled=True)
    positions, flat = slot_positions(own_routes, 1, experts)
    lookup = positions[0] * experts + flat[0]
    picked = (
        returned.reshape(slots_each * experts, model)[lookup]
        .astype(jnp.float32)
        .reshape(block_len, 2, model)
    )
    weights = route_weights(own_rows, group_router, expert_router, own_routes)
    return jnp.sum(picked * weights[:, :, None], axis=1).astype(jnp.bfloat16)


def on_device(
    mixer_input,
    mixer_gain,
    pool_in,
    pool_map,
    pool_scale,
    pool_out,
    expert_input,
    expert_gain,
    group_router,
    expert_router,
    routes,
    gate_weight,
    up_weight,
    down_weight,
):
    mixer_output = mixer_half(mixer_input, mixer_gain, pool_in, pool_map, pool_scale, pool_out)
    expert_output = expert_half(
        expert_input,
        expert_gain,
        group_router,
        expert_router,
        routes,
        gate_weight,
        up_weight,
        down_weight,
    )
    return (mixer_output, expert_output)


def solution(mesh):
    return jax.shard_map(
        on_device,
        mesh=mesh,
        in_specs=(
            P("ep", None),
            P(),
            P(None, "tp"),
            P("tp", None, None),
            P("tp"),
            P("tp", None),
            P("ep", None),
            P(),
            P(),
            P(),
            P("ep", None),
            P("ep", None, "tp"),
            P("ep", None, "tp"),
            P("ep", "tp", None),
        ),
        out_specs=(P(("ep", "tp"), None), P(("ep", "tp"), None)),
        check_vma=False,
    )
```

profile of v0, /device:TPU:0, one launch (start us, length us, event | category | flops | bytes accessed | tf_op | source)
XLA Modules:
  0.0 257.5 jit_solution(10104831046113127895)
XLA Ops:
  7.2 1.9 multiply_reduce_fusion
  9.2 2.0 convert_element_type.167
  13.4 9.4 %scatter_fusion = s32[48,8]{0,1:T(8,128)S(1)} fusion(s32[48,8]{0,1:T(8,128)S(1)} %broadcast_in_dim.11, s32[192]{0:T(256)S(1)} %bitcast.87, s32[192]{0:T(256)S(1)} %and_select_fusion.1), kind=kCustom, calls=%fused_computation.2 | custom fusion | bytes 3840 | tf_op jit(solution)/shard_map/scatter | solution.py:91
  23.1 1.3 fusion.23
  24.4 2.5 gather_fusion
  26.8 1.8 copy_select_fusion
  28.7 44.1 %all_to_all.10 = bf16[48,8,2048]{2,0,1:T(8,128)(2,1)S(1)} all-to-all(bf16[48,8,2048]{2,0,1:T(8,128)(2,1)S(1)} %copy_select_fusion), channel_id=1, replica_groups=mesh['ep'=8,'tp'=4] {'ep'}, dimensions={1} | all-to-all | bytes 3145728 | tf_op jit(solution)/shard_map/all_to_all | solution.py:115
  72.8 2.0 copy.38
  75.1 45.3 %all-gather.2.cloned.1.call-done = bf16[192,8,2048]{2,1,0:T(8,128)(2,1)} async-done(((bf16[48,8,2048]{2,1,0:T(8,128)(2,1)}), bf16[192,8,2048]{2,1,0:T(8,128)(2,1)}) %all-gather.2.cloned.1.call-update) | async-done | bytes 6291472 | tf_op jit(solution)/shard_map/all_gather | solution.py:116
  120.3 5.8 %fusion.20 = f32[192,8,256]{2,1,0:T(8,128)} fusion(bf16[192,8,2048]{2,1,0:T(8,128)(2,1)} %all-gather.2.cloned.1.call-done, bf16[1,2048,256]{2,1,0:T(8,128)(2,1)S(1)} %copy-done.8), kind=kOutput, calls=%fused_computation.35 | convolution fusion | flops 1610612736 | bytes 8912896 | tf_op jit(solution)/shard_map/csed,edh->cseh/dot_general | solution.py:121
  126.1 12.2 %convolution_convert_fusion = bf16[192,8,2048]{2,1,0:T(8,128)(2,1)} fusion(bf16[192,8,2048]{2,1,0:T(8,128)(2,1)} %all-gather.2.cloned.1.call-done, f32[192,8,256]{2,1,0:T(8,128)} %fusion.20, bf16[1,256,2048]{2,1,0:T(8,128)(2,1)S(1)} %copy-done, bf16[1,2048,256]{2,1,0:T(8,128)(2,1)S(1)} %copy-done.9), kind=kOutput, calls=%fused_computation.5 | convolution fusion | flops 3226730496 | bytes 16252928 | tf_op jit(solution)/shard_map/cseh,ehd->csed/dot_general | solution.py:124
  139.1 0.9 copy-done.2
  142.0 3.4 %collective-permute-start = (bf16[15,256]{1,0:T(8,128)(2,1)S(1)}, bf16[15,256]{1,0:T(8,128)(2,1)S(1)}, u32[]{:S(2)}, u32[]{:S(2)}) collective-permute-start(bf16[15,256]{1,0:T(8,128)(2,1)S(1)} %slice.103), channel_id=1, source_target_pairs={{0,4},{4,8},{8,12},{12,16},{16,20},{20,24},{24,28},{1,5},{5,9},{9,... | collective-permute-start | bytes 23048 | tf_op jit(solution)/shard_map/ppermute | solution.py:13
  145.5 1.2 collective-permute-done
  146.7 1.0 maximum_convert_fusion
  147.8 4.8 %convolution_convert_fusion.1 = bf16[512,2048]{1,0:T(8,128)(2,1)} fusion(bf16[256,2048]{1,0:T(8,128)(2,1)} %param.19, f32[256]{0:T(256)S(1)} %convert_element_type.163, f32[527,256]{1,0:T(8,128)S(1)} %maximum_convert_fusion, f32[512]{0:T(512)S(1)} %minimum_convert_fusion, f32[]{:T(128)S(6)} %convert_element_type.160, f32[]{:T(128)S(6)} %convert_element_type.159, ...), kind=kOutput, calls=%fused_computation.10 | convolution fusion | flops 609746944 | bytes 11668544 | tf_op jit(solution)/shard_map/dot_general | solution.py:68
  152.6 44.8 %reduce-scatter.5.cloned.1.call-done = bf16[48,8,2048]{2,1,0:T(8,128)(2,1)} async-done(((bf16[192,8,2048]{2,1,0:T(8,128)(2,1)}), bf16[48,8,2048]{2,1,0:T(8,128)(2,1)}) %reduce-scatter.5.cloned.1.call-update) | async-done | bytes 1572880 | tf_op jit(solution)/shard_map/reduce_scatter | solution.py:125
  197.4 3.4 %copy.39 = bf16[48,8,2048]{2,0,1:T(8,128)(2,1)} copy(bf16[48,8,2048]{2,1,0:T(8,128)(2,1)} %reduce-scatter.5.cloned.1.call-done) | data formatting | bytes 3145728 | tf_op jit(solution)/shard_map/reduce_scatter | solution.py:125
  200.8 5.6 %all-to-all-start.1 = ((bf16[48,8,2048]{2,0,1:T(8,128)(2,1)}), bf16[48,8,2048]{2,0,1:T(8,128)(2,1)}, u32[]{:S(2)}, u32[]{:S(2)}) async-start(bf16[48,8,2048]{2,0,1:T(8,128)(2,1)} %copy.39), calls=%async_computation.3 | async-start | bytes 3145728 | tf_op jit(solution)/shard_map/all_to_all | solution.py:131
  207.6 35.9 %all-to-all-done.1 = bf16[48,8,2048]{2,0,1:T(8,128)(2,1)} async-done(((bf16[48,8,2048]{2,0,1:T(8,128)(2,1)}), bf16[48,8,2048]{2,0,1:T(8,128)(2,1)}, u32[]{:S(2)}, u32[]{:S(2)}) %all-to-all-start.1) | async-done | bytes 1572896 | tf_op jit(solution)/shard_map/all_to_all | solution.py:131
  243.4 2.3 copy.44
  245.7 1.1 gather_fusion.1
  246.9 1.0 reshape.522
  247.8 3.1 %multiply_reduce_fusion.1 = bf16[96,2048]{1,0:T(8,128)(2,1)} fusion(f32[96,2,2048]{2,1,0:T(2,128)S(1)} %reshape.522, f32[96,2]{1,0:T(8,128)S(1)} %copy.41), kind=kLoop, calls=%fused_computation.23 | loop fusion | flops 589824 | bytes 1966848 | tf_op jit(solution)/shard_map/reduce_sum | solution.py:140
  (69 shorter events, 6.4 us)
Async XLA Ops:
  7.2 119.0 %copy-start = (bf16[1,256,2048]{2,1,0:T(8,128)(2,1)S(1)}, bf16[1,256,2048]{2,1,0:T(8,128)(2,1)}, u32[]{:S(2)}) copy-start(bf16[1,256,2048]{2,1,0:T(8,128)(2,1)} %param.27) | copy-start | bytes 3145732
  7.2 2.0 copy-start.1
  7.2 113.1 %all-gather.2.cloned.1.call-start = ((), (), s32[]{:S(2)}) async-start(), calls=%async_computation.5 | async-start | bytes 7864320 | tf_op jit(solution)/shard_map/all_gather | solution.py:116
  11.2 11.7 %copy-start.6 = (bf16[2048]{0:T(1024)(128)(2,1)S(1)}, bf16[2048]{0:T(1024)(128)(2,1)}, u32[]{:S(2)}) copy-start(bf16[2048]{0:T(1024)(128)(2,1)} %param.21) | copy-start | bytes 12292
  74.8 45.5 %copy-start.8 = (bf16[1,2048,256]{2,1,0:T(8,128)(2,1)S(1)}, bf16[1,2048,256]{2,1,0:T(8,128)(2,1)}, u32[]{:S(2)}) copy-start(bf16[1,2048,256]{2,1,0:T(8,128)(2,1)} %param.25) | copy-start | bytes 3145732
  74.8 51.3 %copy-start.9 = (bf16[1,2048,256]{2,1,0:T(8,128)(2,1)S(1)}, bf16[1,2048,256]{2,1,0:T(8,128)(2,1)}, u32[]{:S(2)}) copy-start(bf16[1,2048,256]{2,1,0:T(8,128)(2,1)} %param.26) | copy-start | bytes 3145732
  74.8 122.6 %reduce-scatter.5.cloned.1.call-start = ((), (), s32[]{:S(2)}) async-start(), calls=%async_computation.6 | async-start | bytes 7864320 | tf_op jit(solution)/shard_map/reduce_scatter | solution.py:125
  138.4 0.7 copy-start.7
  138.4 1.6 copy-start.2
  138.4 112.6 %reduce-scatter.3.cloned.1.call-start = ((), (), s32[]{:S(2)}) async-start(), calls=%async_computation.4 | async-start | bytes 2621440 | tf_op jit(solution)/shard_map/reduce_scatter | solution.py:67
  139.1 1.4 copy-start.10
  140.5 5.0 %copy-start.11 = (bf16[256]{0:T(256)(128)(2,1)S(1)}, bf16[256]{0:T(256)(128)(2,1)}, u32[]{:S(2)}) copy-start(bf16[256]{0:T(256)(128)(2,1)} %param.18) | copy-start | bytes 1540
  141.3 0.7 copy-start.3
  142.0 4.7 %collective-permute-start = (bf16[15,256]{1,0:T(8,128)(2,1)S(1)}, bf16[15,256]{1,0:T(8,128)(2,1)S(1)}, u32[]{:S(2)}, u32[]{:S(2)}) collective-permute-start(bf16[15,256]{1,0:T(8,128)(2,1)S(1)} %slice.103), channel_id=1, source_target_pairs={{0,4},{4,8},{8,12},{12,16},{16,20},{20,24},{24,28},{1,5},{5,9},{9,... | collective-permute-start | bytes 23048 | tf_op jit(solution)/shard_map/ppermute | solution.py:13
  200.8 5.7 %copy-start.5 = (bf16[2048,4]{0,1:T(4,128)(2,1)S(1)}, bf16[2048,4]{0,1:T(4,128)(2,1)}, u32[]{:S(2)}) copy-start(bf16[2048,4]{0,1:T(4,128)(2,1)} %param.22) | copy-start | bytes 49156
  200.8 5.9 %copy-start.4 = (bf16[2048,8]{0,1:T(8,128)(2,1)S(1)}, bf16[2048,8]{0,1:T(8,128)(2,1)}, u32[]{:S(2)}) copy-start(bf16[2048,8]{0,1:T(8,128)(2,1)} %param.23) | copy-start | bytes 98308
  200.8 42.6 %all-to-all-start.1 = ((bf16[48,8,2048]{2,0,1:T(8,128)(2,1)}), bf16[48,8,2048]{2,0,1:T(8,128)(2,1)}, u32[]{:S(2)}, u32[]{:S(2)}) async-start(bf16[48,8,2048]{2,0,1:T(8,128)(2,1)} %copy.39), calls=%async_computation.3 | async-start | bytes 3145728 | tf_op jit(solution)/shard_map/all_to_all | solution.py:131
Sparse Core Ops, SparseCore 0:
  74.9 45.3 all-gather.1
  138.5 58.8 reduce-scatter.4
  200.5 31.1 reduce-scatter.2
where the time goes:
time: 258 us
  waiting for transfers between devices  127 us (49%)
  blocking collectives  44.1 us (17%)
  local copies, waits for them, and re-layouts  25.7 us (10%)
  matrix products  24.5 us (9%)
  between operations  14.1 us (5%)
  other arithmetic  12.6 us (5%)
  starting transfers between devices  9.32 us (4%)
    all_gather x1, waiting for transfers between devices, expert_half(): received = lax.all_gather(arrived, 'tp', axis=0, tiled=True)  45.3 us
    reduce_scatter x1, waiting for transfers between devices, expert_half(): lax.psum_scatter(result.reshape(lax.axis_size('tp') * slots_each, -1, mod...  44.8 us
    all_to_all x1, blocking collectives, expert_half(): lax.all_to_all(sending, 'ep', split_axis=1, concat_axis=1, tiled=True)  44.1 us
    all_to_all x1, waiting for transfers between devices, expert_half(): lax.all_to_all(summed, 'ep', split_axis=1, concat_axis=1, tiled=True)  35.9 us
    dot_general x1, matrix products, expert_half(): jnp.einsum('cseh,ehd->csed', hidden, down_weight, preferred_element_type=...  12.2 us
    scatter x1, local copies, waits for them, and re-layouts, dispatch_rows(): table.at[slot_index.reshape(-1), flat.reshape(-1)]  9.38 us
    dot_general x1, matrix products, expert_half(): jnp.einsum('csed,edh->cseh', portion, gate_weight, preferred_element_type...  5.78 us
    all_to_all x1, starting transfers between devices, expert_half(): lax.all_to_all(summed, 'ep', split_axis=1, concat_axis=1, tiled=True)  5.65 us
  transfers between devices with their start and end apart: 5, of which 4 were waited for; matrix products, arithmetic and copies ran while one was open for 7% of the time, Pallas kernels for 0%

commit v1 on v0

--- a/solution.py
+++ b/solution.py
@@ -128,7 +128,12 @@
         scatter_dimension=0,
         tiled=True,
     )
-    returned = lax.all_to_all(summed, "ep", split_axis=1, concat_axis=1, tiled=True)
+    returned = jnp.concatenate(
+        lax.all_to_all(
+            jnp.stack(jnp.split(summed, lax.axis_size("ep"), axis=1), axis=0), "ep", 0, 0
+        ),
+        1,
+    )
     positions, flat = slot_positions(own_routes, 1, experts)
     lookup = positions[0] * experts + flat[0]
     picked = (

time: 258 us -> 274 us (1.062)
  local copies, waits for them, and re-layouts: 25.7 us -> 41.7 us
    split x0 -> x1, local copies, waits for them, and re-layouts: none -> 9.73 us  [expert_half(): jnp.split(summed, lax.axis_size('ep'), axis=1)]
    unnamed x24 -> x33, local copies, waits for them, and re-layouts: 2.27 us -> 8.95 us
    reduce_scatter x1 -> x0, local copies, waits for them, and re-layouts: 3.43 us -> none  [expert_half(): lax.psum_scatter(result.reshape(lax.axis_size('tp') * slots_each, -1, mod...]
  transfers between devices with their start and end apart: 5 -> 5, of which waited for: 4 -> 4; matrix products, arithmetic and copies ran while one was open for 7% -> 12% of each run, Pallas kernels for 0% -> 0%
where the time goes in v1:
time: 274 us; the launch traced here: 273 us
  waiting for transfers between devices  127 us (46%)
  blocking collectives  44.1 us (16%)
  local copies, waits for them, and re-layouts  41.7 us (15%)
  matrix products  24.5 us (9%)
  between operations  14.1 us (5%)
  other arithmetic  12.4 us (5%)
  starting transfers between devices  9.54 us (3%)
    all_gather x1, waiting for transfers between devices, expert_half(): received = lax.all_gather(arrived, 'tp', axis=0, tiled=True)  45.3 us
    reduce_scatter x1, waiting for transfers between devices, expert_half(): lax.psum_scatter(result.reshape(lax.axis_size('tp') * slots_each, -1, mod...  44.8 us
    all_to_all x1, blocking collectives, expert_half(): lax.all_to_all(sending, 'ep', split_axis=1, concat_axis=1, tiled=True)  44.1 us
    all_to_all x1, waiting for transfers between devices, expert_half(): lax.all_to_all(jnp.stack(jnp.split(summed, lax.axis_size('ep'), axis=1),...  35.8 us
    dot_general x1, matrix products, expert_half(): jnp.einsum('cseh,ehd->csed', hidden, down_weight, preferred_element_type=...  12.2 us
    split x1, local copies, waits for them, and re-layouts, expert_half(): jnp.split(summed, lax.axis_size('ep'), axis=1)  9.73 us
    scatter x1, local copies, waits for them, and re-layouts, dispatch_rows(): table.at[slot_index.reshape(-1), flat.reshape(-1)]  9.38 us
    unnamed x33, local copies, waits for them, and re-layouts  8.95 us
  transfers between devices with their start and end apart: 5, of which 4 were waited for; matrix products, arithmetic and copies ran while one was open for 12% of the time, Pallas kernels for 0%

profile of v1, /device:TPU:0, one launch (start us, length us, event | category | flops | bytes accessed | tf_op | source)
XLA Modules:
  0.0 273.2 jit_solution(870969157352661302)
XLA Ops:
  8.5 1.8 multiply_reduce_fusion
  10.3 2.0 convert_element_type.167
  13.4 9.4 %scatter_fusion = s32[48,8]{0,1:T(8,128)S(1)} fusion(s32[48,8]{0,1:T(8,128)S(1)} %broadcast_in_dim.11, s32[192]{0:T(256)S(1)} %bitcast.104, s32[192]{0:T(256)S(1)} %and_select_fusion.1), kind=kCustom, calls=%fused_computation.2 | custom fusion | bytes 3840 | tf_op jit(solution)/shard_map/scatter | solution.py:91
  23.1 1.3 fusion.23
  24.4 2.5 gather_fusion
  26.8 1.8 copy_select_fusion
  28.7 44.1 %all_to_all.10 = bf16[48,8,2048]{2,0,1:T(8,128)(2,1)S(1)} all-to-all(bf16[48,8,2048]{2,0,1:T(8,128)(2,1)S(1)} %copy_select_fusion), channel_id=1, replica_groups=mesh['ep'=8,'tp'=4] {'ep'}, dimensions={1} | all-to-all | bytes 3145728 | tf_op jit(solution)/shard_map/all_to_all | solution.py:115
  72.8 2.0 copy.115
  75.0 45.3 %all-gather.2.cloned.1.call-done = bf16[192,8,2048]{2,1,0:T(8,128)(2,1)} async-done(((bf16[48,8,2048]{2,1,0:T(8,128)(2,1)}), bf16[192,8,2048]{2,1,0:T(8,128)(2,1)}) %all-gather.2.cloned.1.call-update) | async-done | bytes 6291472 | tf_op jit(solution)/shard_map/all_gather | solution.py:116
  120.3 5.8 %fusion.20 = f32[192,8,256]{2,1,0:T(8,128)} fusion(bf16[192,8,2048]{2,1,0:T(8,128)(2,1)} %all-gather.2.cloned.1.call-done, bf16[1,2048,256]{2,1,0:T(8,128)(2,1)S(1)} %copy-done.9), kind=kOutput, calls=%fused_computation.35 | convolution fusion | flops 1610612736 | bytes 8912896 | tf_op jit(solution)/shard_map/csed,edh->cseh/dot_general | solution.py:121
  126.1 12.2 %convolution_convert_fusion = bf16[192,8,2048]{2,1,0:T(8,128)(2,1)} fusion(bf16[192,8,2048]{2,1,0:T(8,128)(2,1)} %all-gather.2.cloned.1.call-done, f32[192,8,256]{2,1,0:T(8,128)} %fusion.20, bf16[1,256,2048]{2,1,0:T(8,128)(2,1)S(1)} %copy-done, bf16[1,2048,256]{2,1,0:T(8,128)(2,1)S(1)} %copy-done.10), kind=kOutput, calls=%fused_computation.5 | convolution fusion | flops 3226730496 | bytes 16252928 | tf_op jit(solution)/shard_map/cseh,ehd->csed/dot_general | solution.py:124
  142.0 3.6 %collective-permute-start = (bf16[15,256]{1,0:T(8,128)(2,1)S(1)}, bf16[15,256]{1,0:T(8,128)(2,1)S(1)}, u32[]{:S(2)}, u32[]{:S(2)}) collective-permute-start(bf16[15,256]{1,0:T(8,128)(2,1)S(1)} %slice.103), channel_id=1, source_target_pairs={{0,4},{4,8},{8,12},{12,16},{16,20},{20,24},{24,28},{1,5},{5,9},{9,... | collective-permute-start | bytes 23048 | tf_op jit(solution)/shard_map/ppermute | solution.py:13
  145.7 1.0 collective-permute-done
  146.7 1.0 maximum_convert_fusion
  147.7 4.8 %convolution_convert_fusion.1 = bf16[512,2048]{1,0:T(8,128)(2,1)} fusion(bf16[256,2048]{1,0:T(8,128)(2,1)} %param.19, f32[256]{0:T(256)S(1)} %convert_element_type.163, f32[527,256]{1,0:T(8,128)S(1)} %maximum_convert_fusion, f32[512]{0:T(512)S(1)} %minimum_convert_fusion, f32[]{:T(128)S(6)} %convert_element_type.160, f32[]{:T(128)S(6)} %convert_element_type.159, ...), kind=kOutput, calls=%fused_computation.10 | convolution fusion | flops 609746944 | bytes 11668544 | tf_op jit(solution)/shard_map/dot_general | solution.py:68
  152.6 44.8 %reduce-scatter.5.cloned.1.call-done = bf16[48,8,2048]{2,1,0:T(8,128)(2,1)} async-done(((bf16[192,8,2048]{2,1,0:T(8,128)(2,1)}), bf16[48,8,2048]{2,1,0:T(8,128)(2,1)}) %reduce-scatter.5.cloned.1.call-update) | async-done | bytes 1572880 | tf_op jit(solution)/shard_map/reduce_scatter | solution.py:125
  197.4 9.7 %fusion.55 = (bf16[48,1,2048]{2,1,0:T(2,128)(2,1)S(1)}, bf16[48,1,2048]{2,1,0:T(2,128)(2,1)S(1)}, bf16[48,1,2048]{2,1,0:T(2,128)(2,1)S(1)}, bf16[48,1,2048]{2,1,...) fusion(bf16[48,8,2048]{2,1,0:T(8,128)(2,1)} %reduce-scatter.5.c, ...), kind=kLoop, calls=%fused_computation.126 | loop fusion | bytes 3145728 | tf_op jit(solution)/shard_map/split | solution.py:133
  213.5 5.6 %all-to-all-start.1 = ((bf16[8,48,1,2048]{3,1,2,0:T(8,128)(2,1)}), bf16[8,48,1,2048]{3,1,2,0:T(8,128)(2,1)S(1)}, u32[]{:S(2)}, u32[]{:S(2)}) async-start(bf16[8,48,1,2048]{3,1,2,0:T(8,128)(2,1)} %bitcast_dynamic-update-slice_fusion), calls=%async_computation.3 | async-start | bytes 3145728 | tf_op jit(solution)/shard_map/all_to_all | solution.py:132
  220.2 35.8 %all-to-all-done.1 = bf16[8,48,1,2048]{3,1,2,0:T(8,128)(2,1)S(1)} async-done(((bf16[8,48,1,2048]{3,1,2,0:T(8,128)(2,1)}), bf16[8,48,1,2048]{3,1,2,0:T(8,128)(2,1)S(1)}, u32[]{:S(2)}, u32[]{:S(2)}) %all-to-all-start.1) | async-done | bytes 1572896 | tf_op jit(solution)/shard_map/all_to_all | solution.py:132
  256.0 1.2 copy-done.1
  257.1 2.3 copy.136
  259.4 2.0 gather_fusion.1
  261.4 2.1 reshape.522
  263.6 3.1 %multiply_reduce_fusion.1 = bf16[96,2048]{1,0:T(8,128)(2,1)} fusion(f32[96,2,2048]{2,1,0:T(2,128)S(1)} %reshape.522, f32[96,2]{1,0:T(8,128)S(1)} %copy.117), kind=kLoop, calls=%fused_computation.23 | loop fusion | flops 589824 | bytes 1966848 | tf_op jit(solution)/shard_map/reduce_sum | solution.py:145
  (79 shorter events, 13.8 us)
Async XLA Ops:
  7.2 118.9 %copy-start = (bf16[1,256,2048]{2,1,0:T(8,128)(2,1)S(1)}, bf16[1,256,2048]{2,1,0:T(8,128)(2,1)}, u32[]{:S(2)}) copy-start(bf16[1,256,2048]{2,1,0:T(8,128)(2,1)} %param.27) | copy-start | bytes 3145732
  7.2 3.2 %copy-start.2 = (bf16[384,2048]{1,0:T(8,128)(2,1)S(1)}, bf16[384,2048]{1,0:T(8,128)(2,1)}, u32[]{:S(2)}) copy-start(bf16[384,2048]{1,0:T(8,128)(2,1)} %param.20) | copy-start | bytes 4718596
  7.2 113.1 %all-gather.2.cloned.1.call-start = ((), (), s32[]{:S(2)}) async-start(), calls=%async_computation.5 | async-start | bytes 7864320 | tf_op jit(solution)/shard_map/all_gather | solution.py:116
  12.4 10.7 %copy-start.7 = (bf16[2048]{0:T(1024)(128)(2,1)S(1)}, bf16[2048]{0:T(1024)(128)(2,1)}, u32[]{:S(2)}) copy-start(bf16[2048]{0:T(1024)(128)(2,1)} %param.21) | copy-start | bytes 12292
  74.8 45.5 %copy-start.9 = (bf16[1,2048,256]{2,1,0:T(8,128)(2,1)S(1)}, bf16[1,2048,256]{2,1,0:T(8,128)(2,1)}, u32[]{:S(2)}) copy-start(bf16[1,2048,256]{2,1,0:T(8,128)(2,1)} %param.25) | copy-start | bytes 3145732
  74.8 51.3 %copy-start.10 = (bf16[1,2048,256]{2,1,0:T(8,128)(2,1)S(1)}, bf16[1,2048,256]{2,1,0:T(8,128)(2,1)}, u32[]{:S(2)}) copy-start(bf16[1,2048,256]{2,1,0:T(8,128)(2,1)} %param.26) | copy-start | bytes 3145732
  74.8 122.6 %reduce-scatter.5.cloned.1.call-start = ((), (), s32[]{:S(2)}) async-start(), calls=%async_computation.6 | async-start | bytes 7864320 | tf_op jit(solution)/shard_map/reduce_scatter | solution.py:125
  138.4 0.7 copy-start.8
  138.4 1.6 copy-start.3
  138.4 128.3 %reduce-scatter.3.cloned.1.call-start = ((), (), s32[]{:S(2)}) async-start(), calls=%async_computation.4 | async-start | bytes 2621440 | tf_op jit(solution)/shard_map/reduce_scatter | solution.py:67
  139.0 1.4 copy-start.11
  140.5 5.2 %copy-start.12 = (bf16[256]{0:T(256)(128)(2,1)S(1)}, bf16[256]{0:T(256)(128)(2,1)}, u32[]{:S(2)}) copy-start(bf16[256]{0:T(256)(128)(2,1)} %param.18) | copy-start | bytes 1540
  141.3 0.7 copy-start.4
  142.0 4.7 %collective-permute-start = (bf16[15,256]{1,0:T(8,128)(2,1)S(1)}, bf16[15,256]{1,0:T(8,128)(2,1)S(1)}, u32[]{:S(2)}, u32[]{:S(2)}) collective-permute-start(bf16[15,256]{1,0:T(8,128)(2,1)S(1)} %slice.103), channel_id=1, source_target_pairs={{0,4},{4,8},{8,12},{12,16},{16,20},{20,24},{24,28},{1,5},{5,9},{9,... | collective-permute-start | bytes 23048 | tf_op jit(solution)/shard_map/ppermute | solution.py:13
  213.5 5.7 %copy-start.6 = (bf16[2048,4]{0,1:T(4,128)(2,1)S(1)}, bf16[2048,4]{0,1:T(4,128)(2,1)}, u32[]{:S(2)}) copy-start(bf16[2048,4]{0,1:T(4,128)(2,1)} %param.22) | copy-start | bytes 49156
  213.5 5.9 %copy-start.5 = (bf16[2048,8]{0,1:T(8,128)(2,1)S(1)}, bf16[2048,8]{0,1:T(8,128)(2,1)}, u32[]{:S(2)}) copy-start(bf16[2048,8]{0,1:T(8,128)(2,1)} %param.23) | copy-start | bytes 98308
  213.5 42.5 %all-to-all-start.1 = ((bf16[8,48,1,2048]{3,1,2,0:T(8,128)(2,1)}), bf16[8,48,1,2048]{3,1,2,0:T(8,128)(2,1)S(1)}, u32[]{:S(2)}, u32[]{:S(2)}) async-start(bf16[8,48,1,2048]{3,1,2,0:T(8,128)(2,1)} %bitcast_dynamic-update-slice_fusion), calls=%async_computation.3 | async-start | bytes 3145728 | tf_op jit(solution)/shard_map/all_to_all | solution.py:132
  256.0 1.2 copy-start.1
Sparse Core Ops, SparseCore 0:
  74.9 45.3 all-gather.1
  138.5 58.8 reduce-scatter.4
  200.5 31.1 reduce-scatter.2
